TPU v7x, 32 devices: a whole 2x2x4 slice. The times are simulated.
32 devices in a mesh: gr: 2 (over x), fs: 8 (over z, y), tp: 2 (over core).
Axes of the slice: x: 2, y: 2, z: 4, core: 2. Of those that a mesh axis runs over, the one named last changes fastest.
Arguments:
- prompt: bfloat16 [3072, 2048], P(('gr', 'fs', 'tp')), may hold values from -6 to 6
- norm_first: float32 [2048], P(('gr', 'fs')), may hold values from 0.1 to 1.9
- gate_first: float32 [2048, 5632], P(('gr', 'fs'), 'tp'), may hold values from -6 to 6
- up_first: float32 [2048, 5632], P(('gr', 'fs'), 'tp'), may hold values from -6 to 6
- down_first: float32 [2048, 5632], P(('gr', 'fs'), 'tp'), may hold values from -6 to 6
- norm_second: float32 [2048], P(('gr', 'fs')), may hold values from 0.1 to 1.9
- gate_second: float32 [2048, 5632], P(('gr', 'fs'), 'tp'), may hold values from -6 to 6
- up_second: float32 [2048, 5632], P(('gr', 'fs'), 'tp'), may hold values from -6 to 6
- down_second: float32 [2048, 5632], P(('gr', 'fs'), 'tp'), may hold values from -6 to 6
Outputs:
- served_gate_first: bfloat16 [2048, 5632], P(None, 'fs')
- served_up_first: bfloat16 [2048, 5632], P(None, 'fs')
- served_down_first: bfloat16 [2048, 5632], P(None, 'fs')
- served_gate_second: bfloat16 [2048, 5632], P(None, 'fs')
- served_up_second: bfloat16 [2048, 5632], P(None, 'fs')
- served_down_second: bfloat16 [2048, 5632], P(None, 'fs')
- result: bfloat16 [3072, 2048], P(('gr', 'fs', 'tp'))
All inputs are finite; a program needn't handle non-finite values.
Results may differ from a plain program's by a relative error of at most 0.015.
Values may be sent and summed in bfloat16 or wider, within the bound.
A program may use at most 128 MiB of HBM per device.

v0:
```python
import jax
import jax.numpy as jnp
from jax import lax
from jax.sharding import PartitionSpec as P

D = 2048
FF = 5632
EPS = 1e-06


def fold_rows(gain, weight):
    return (gain[:, None] * weight).astype(jnp.bfloat16)


def relayout(stacked):
    moved = lax.all_to_all(
        lax.all_to_all(stacked, "tp", split_axis=1, concat_axis=2, tiled=True),
        "fs",
        split_axis=2,
        concat_axis=1,
        tiled=True,
    )
    whole = lax.all_gather(moved, ("gr", "tp"), axis=1, tiled=True)
    matrices = stacked.shape[0]
    block_width = moved.shape[2]
    gr_size = lax.axis_size("gr")
    tp_size = lax.axis_size("tp")
    fs_size = lax.axis_size("fs")
    sub_rows = stacked.shape[1] // tp_size
    shaped = whole.reshape(matrices, gr_size, tp_size, fs_size, sub_rows, block_width)
    return shaped.transpose(0, 1, 3, 2, 4, 5).reshape(
        matrices, gr_size * fs_size * tp_size * sub_rows, block_width
    )


def half_step(residual, weights):
    gate_weight = weights[0]
    up_weight = weights[1]
    down_weight = weights[2]
    resid_f = residual.astype(jnp.float32)
    normed = (
        resid_f * lax.rsqrt(jnp.mean(resid_f * resid_f, axis=-1, keepdims=True) + EPS)
    ).astype(jnp.bfloat16)
    in_scale = D ** (-0.5)
    out_scale = FF ** (-0.5)
    tokens_in = lax.all_gather(normed, "fs", axis=0, tiled=True)
    gate_pre = jnp.dot(tokens_in, gate_weight, preferred_element_type=jnp.float32) * in_scale
    up_pre = jnp.dot(tokens_in, up_weight, preferred_element_type=jnp.float32) * in_scale
    hidden = (jax.nn.silu(gate_pre) * up_pre).astype(jnp.bfloat16)
    branch = lax.psum_scatter(
        (
            lax.dot_general(
                hidden, down_weight, (((1,), (1,)), ((), ())), preferred_element_type=jnp.float32
            )
            * out_scale
        ).astype(jnp.bfloat16),
        "fs",
        scatter_dimension=0,
        tiled=True,
    ).astype(jnp.float32)
    return (resid_f + 0.5 * branch).astype(jnp.bfloat16)


def on_device(
    prompt,
    norm_first,
    gate_first,
    up_first,
    down_first,
    norm_second,
    gate_second,
    up_second,
    down_second,
):
    first_set = jnp.stack(
        [
            fold_rows(norm_first, gate_first),
            fold_rows(norm_first, up_first),
            down_first.astype(jnp.bfloat16),
        ]
    )
    second_set = jnp.stack(
        [
            fold_rows(norm_second, gate_second),
            fold_rows(norm_second, up_second),
            down_second.astype(jnp.bfloat16),
        ]
    )
    served_first = relayout(first_set)
    middle = half_step(prompt, served_first)
    served_second = relayout(second_set)
    result = half_step(middle, served_second)
    return (
        served_first[0],
        served_first[1],
        served_first[2],
        served_second[0],
        served_second[1],
        served_second[2],
        result,
    )


def solution(mesh):
    in_specs = (
        P(("gr", "fs", "tp"), None),
        P(("gr", "fs")),
        P(("gr", "fs"), "tp"),
        P(("gr", "fs"), "tp"),
        P(("gr", "fs"), "tp"),
        P(("gr", "fs")),
        P(("gr", "fs"), "tp"),
        P(("gr", "fs"), "tp"),
        P(("gr", "fs"), "tp"),
    )
    out_specs = (
        P(None, "fs"),
        P(None, "fs"),
        P(None, "fs"),
        P(None, "fs"),
        P(None, "fs"),
        P(None, "fs"),
        P(("gr", "fs", "tp"), None),
    )
    return jax.shard_map(
        on_device, mesh=mesh, in_specs=in_specs, out_specs=out_specs, check_vma=False
    )
```

profile of v0, /device:TPU:0, one launch (start us, length us, event | category | flops | bytes accessed | tf_op | source)
XLA Modules:
  0.0 607.6 jit_solution(7273351563624397723)
XLA Ops:
  7.2 0.0 all-gather.5.cloned.1.call-start
  7.2 2.5 fusion.6
  9.7 0.2 pad_maximum_fusion
  10.0 1.9 copy.52
  11.8 6.0 all_to_all.72
  17.9 2.6 copy.77
  20.5 10.8 %copy.72 = bf16[3,64,2,2816]{1,0,3,2:T(4,128)(2,1)} copy(bf16[3,64,2,2816]{3,2,1,0:T(2,128)(2,1)S(1)} %bitcast.78) | data formatting | bytes 4325376 | tf_op jit(solution)/shard_map/all_to_all | solution.py:17
  31.3 7.1 %reshape.54 = bf16[8,2,67584]{2,1,0:T(2,128)(2,1)S(1)} reshape(bf16[5632,3,64]{2,1,0:T(4,128)(2,1)} %bitcast.56) | data formatting | bytes 4325376
  38.4 57.7 %all_to_all.73 = bf16[8,2,67584]{2,1,0:T(2,128)(2,1)} all-to-all(bf16[8,2,67584]{2,1,0:T(2,128)(2,1)S(1)} %reshape.54), channel_id=1, replica_groups=mesh['gr'=2,'fs'=8,'tp'=2] {'fs'}, dimensions={0} | all-to-all | bytes 4325376 | tf_op jit(solution)/shard_map/all_to_all | solution.py:16
  96.1 8.0 %reshape.55 = bf16[5632,3,64]{2,1,0:T(4,128)(2,1)} reshape(bf16[8,2,67584]{2,1,0:T(2,128)(2,1)} %all_to_all.73) | data formatting | bytes 4325376
  104.1 9.4 %copy.55 = bf16[3,64,8,704]{3,1,2,0:T(8,128)(2,1)} copy(bf16[3,64,8,704]{1,0,3,2:T(4,128)(2,1)} %bitcast.57) | data formatting | bytes 4325376 | tf_op jit(solution)/shard_map/all_to_all | solution.py:16
  113.5 0.0 all-gather.5.cloned.1.call-update
  113.5 0.0 all-gather.9.cloned.1.call-start
  113.6 0.0 copy-done.1
  113.6 0.2 fusion
  113.8 0.9 fusion.1
  114.7 0.0 all-gather.9.cloned.1.call-update
  114.7 0.3 reduce-scatter.3.cloned.1.call-start
  115.0 61.3 %all-gather.5.cloned.1.call-done = bf16[3,2048,704]{2,1,0:T(8,128)(2,1)} async-done(((bf16[3,512,704]{2,1,0:T(8,128)(2,1)}), bf16[3,2048,704]{2,1,0:T(8,128)(2,1)}) %all-gather.5.cloned.1.call-update) | async-done | bytes 8650768 | tf_op jit(solution)/shard_map/all_gather | solution.py:23
  176.3 4.1 fusion.15
  180.4 0.3 copy.56
  180.8 1.9 copy.57
  182.6 1.8 copy.58
  184.5 54.6 %all-gather.9.cloned.1.call-done = bf16[768,2048]{1,0:T(8,128)(2,1)} async-done(((bf16[96,2048]{1,0:T(8,128)(2,1)}), bf16[768,2048]{1,0:T(8,128)(2,1)}) %all-gather.9.cloned.1.call-update) | async-done | bytes 3145744 | tf_op jit(solution)/shard_map/all_gather | solution.py:46
  239.1 5.7 fusion.16
  244.8 12.4 %multiply_convert_fusion.1 = bf16[768,2048]{1,0:T(8,128)(2,1)} fusion(bf16[2048,704]{1,0:T(8,128)(2,1)} %bitcast.64, f32[768,704]{0,1:T(8,128)} %fusion.16, bf16[768,2048]{1,0:T(8,128)(2,1)} %all-gather.9.cloned.1.call-done, bf16[2048,704]{1,0:T(8,128)(2,1)} %bitcast.62), kind=kOutput, calls=%fused_computation.1 | convolution fusion | flops 4436656128 | bytes 14221312 | tf_op jit(solution)/shard_map/dot_general | solution.py:52
  257.2 0.0 reduce-scatter.3.cloned.1.call-update
  257.3 0.5 all-gather.7.cloned.1.call-start
  257.8 0.1 copy-done.2
  257.9 2.5 fusion.8
  260.4 0.2 pad_maximum_fusion.1
  260.6 1.9 copy.59
  262.5 6.0 all_to_all.74
  268.5 3.9 copy.76
  272.5 15.1 %copy.73 = bf16[3,64,2,2816]{1,0,3,2:T(4,128)(2,1)} copy(bf16[3,64,2,2816]{3,2,1,0:T(2,128)(2,1)} %bitcast.79) | data formatting | bytes 4325376 | tf_op jit(solution)/shard_map/all_to_all | solution.py:17
  287.6 8.2 %reshape.56 = bf16[8,2,67584]{2,1,0:T(2,128)(2,1)} reshape(bf16[5632,3,64]{2,1,0:T(4,128)(2,1)} %bitcast.58) | data formatting | bytes 4325376
  295.9 67.8 %all_to_all.75 = bf16[8,2,67584]{2,1,0:T(2,128)(2,1)} all-to-all(bf16[8,2,67584]{2,1,0:T(2,128)(2,1)} %reshape.56), channel_id=1, replica_groups=mesh['gr'=2,'fs'=8,'tp'=2] {'fs'}, dimensions={0} | all-to-all | bytes 4325376 | tf_op jit(solution)/shard_map/all_to_all | solution.py:16
  363.7 8.0 %reshape.57 = bf16[5632,3,64]{2,1,0:T(4,128)(2,1)} reshape(bf16[8,2,67584]{2,1,0:T(2,128)(2,1)} %all_to_all.75) | data formatting | bytes 4325376
  371.6 9.4 %copy.62 = bf16[3,64,8,704]{3,1,2,0:T(8,128)(2,1)} copy(bf16[3,64,8,704]{1,0,3,2:T(4,128)(2,1)} %bitcast.59) | data formatting | bytes 4325376 | tf_op jit(solution)/shard_map/all_to_all | solution.py:16
  381.0 0.0 all-gather.7.cloned.1.call-update
  381.0 0.0 all-gather.11.cloned.1.call-start
  381.1 0.0 reduce-scatter.3.cloned.1.call-done
  381.1 1.3 fusion.3
  382.4 1.9 fusion.4
  384.3 0.0 all-gather.11.cloned.1.call-update
  384.3 0.2 reduce-scatter.5.cloned.1.call-start
  384.5 59.3 %all-gather.7.cloned.1.call-done = bf16[3,2048,704]{2,1,0:T(8,128)(2,1)} async-done(((bf16[3,512,704]{2,1,0:T(8,128)(2,1)}), bf16[3,2048,704]{2,1,0:T(8,128)(2,1)}) %all-gather.7.cloned.1.call-update) | async-done | bytes 8650768 | tf_op jit(solution)/shard_map/all_gather | solution.py:23
  443.8 4.1 fusion.14
  447.9 1.9 copy.63
  449.8 1.9 copy.64
  451.7 1.9 copy.65
  453.6 52.8 %all-gather.11.cloned.1.call-done = bf16[768,2048]{1,0:T(8,128)(2,1)} async-done(((bf16[96,2048]{1,0:T(8,128)(2,1)}), bf16[768,2048]{1,0:T(8,128)(2,1)}) %all-gather.11.cloned.1.call-update) | async-done | bytes 3145744 | tf_op jit(solution)/shard_map/all_gather | solution.py:46
  506.5 6.6 %fusion.17 = f32[768,704]{0,1:T(8,128)} fusion(bf16[768,2048]{1,0:T(8,128)(2,1)} %all-gather.11.cloned.1.call-done, bf16[2048,704]{1,0:T(8,128)(2,1)} %bitcast.66), kind=kOutput, calls=%fused_computation.39 | convolution fusion | flops 2214592512 | bytes 8192000 | tf_op jit(solution)/shard_map/dot_general | solution.py:47
  513.1 12.4 %multiply_convert_fusion = bf16[768,2048]{1,0:T(8,128)(2,1)} fusion(bf16[2048,704]{1,0:T(8,128)(2,1)} %bitcast.70, f32[768,704]{0,1:T(8,128)} %fusion.17, bf16[768,2048]{1,0:T(8,128)(2,1)} %all-gather.11.cloned.1.call-done, bf16[2048,704]{1,0:T(8,128)(2,1)} %bitcast.68), kind=kOutput, calls=%fused_computation | convolution fusion | flops 4436656128 | bytes 14221312 | tf_op jit(solution)/shard_map/dot_general | solution.py:52
  525.5 0.0 reduce-scatter.5.cloned.1.call-update
  525.6 4.6 copy.69
  530.1 4.6 copy.70
  534.7 4.6 copy.71
  539.2 2.7 copy.66
  541.9 4.7 copy.67
  546.7 0.0 copy-done
  546.7 2.7 copy.68
  549.3 49.1 %reduce-scatter.5.cloned.1.call-done = bf16[96,2048]{1,0:T(8,128)(2,1)} async-done(((bf16[768,2048]{1,0:T(8,128)(2,1)}), bf16[96,2048]{1,0:T(8,128)(2,1)}) %reduce-scatter.5.cloned.1.call-update) | async-done | bytes 393232 | tf_op jit(solution)/shard_map/reduce_scatter | solution.py:50
  598.5 2.1 fusion.5
  (5 shorter events, 0.0 us)
Async XLA Ops:
  7.2 169.1 %all-gather.5.cloned.1.call-start = ((), (), s32[]{:S(2)}) async-start(), calls=%async_computation.6 | async-start | bytes 11796480 | tf_op jit(solution)/shard_map/all_gather | solution.py:23
  104.1 9.5 %copy-start.1 = (bf16[96,2048]{1,0:T(8,128)(2,1)S(1)}, bf16[96,2048]{1,0:T(8,128)(2,1)}, u32[]{:S(2)}) copy-start(bf16[96,2048]{1,0:T(8,128)(2,1)} %param.9) | copy-start | bytes 1179652
  113.5 125.6 %all-gather.9.cloned.1.call-start = ((), (), s32[]{:S(2)}) async-start(), calls=%async_computation.8 | async-start | bytes 3538944 | tf_op jit(solution)/shard_map/all_gather | solution.py:46
  114.7 266.4 %reduce-scatter.3.cloned.1.call-start = ((), (), s32[]{:S(2)}) async-start(), calls=%async_computation.9 | async-start | bytes 3538944 | tf_op jit(solution)/shard_map/reduce_scatter | solution.py:50
  257.2 0.7 copy-start.2
  257.3 186.5 %all-gather.7.cloned.1.call-start = ((), (), s32[]{:S(2)}) async-start(), calls=%async_computation.7 | async-start | bytes 11796480 | tf_op jit(solution)/shard_map/all_gather | solution.py:23
  381.0 125.4 %all-gather.11.cloned.1.call-start = ((), (), s32[]{:S(2)}) async-start(), calls=%async_computation.10 | async-start | bytes 3538944 | tf_op jit(solution)/shard_map/all_gather | solution.py:46
  384.3 214.2 %reduce-scatter.5.cloned.1.call-start = ((), (), s32[]{:S(2)}) async-start(), calls=%async_computation.11 | async-start | bytes 3538944 | tf_op jit(solution)/shard_map/reduce_scatter | solution.py:50
  541.9 4.7 copy-start
Sparse Core Ops, SparseCore 0:
  113.6 62.6 all-gather.4
  179.1 60.0 all-gather.8
  257.4 96.6 reduce-scatter.2
  381.2 62.5 all-gather.6
  446.4 60.0 all-gather.10
  525.7 72.7 reduce-scatter.4
where the time goes:
time: 615 us; the launch traced here: 608 us
  waiting for transfers between devices  277 us (45%)
  blocking collectives  138 us (22%)
  local copies, waits for them, and re-layouts  128 us (21%)
  matrix products  37.2 us (6%)
  between operations  14.4 us (2%)
  other arithmetic  11.8 us (2%)
    all_to_all x2, blocking collectives, relayout(): lax.all_to_all(lax.all_to_all(stacked, 'tp', split_axis=1, concat_axis=2,...  126 us
    all_gather x2, waiting for transfers between devices, relayout(): whole = lax.all_gather(moved, ('gr', 'tp'), axis=1, tiled=True)  121 us
    all_gather x2, waiting for transfers between devices, half_step(): tokens_in = lax.all_gather(normed, 'fs', axis=0, tiled=True)  107 us
    unnamed x16, local copies, waits for them, and re-layouts  55.2 us
    reduce_scatter x2, waiting for transfers between devices, half_step(): lax.psum_scatter((lax.dot_general(hidden, down_weight, (((1,), (1,)), (()...  49.1 us
    all_to_all x4, local copies, waits for them, and re-layouts, relayout(): lax.all_to_all(stacked, 'tp', split_axis=1, concat_axis=2, tiled=True)  32.4 us
    dot_general x2, matrix products, half_step(): lax.dot_general(hidden, down_weight, (((1,), (1,)), ((), ())), preferred_...  24.9 us
    all_to_all x2, local copies, waits for them, and re-layouts, relayout(): lax.all_to_all(lax.all_to_all(stacked, 'tp', split_axis=1, concat_axis=2,...  18.8 us
  transfers between devices with their start and end apart: 6, of which 5 were waited for; matrix products, arithmetic and copies ran while one was open for 16% of the time, Pallas kernels for 0%

commit v1 on v0

--- a/solution.py
+++ b/solution.py
@@ -13,12 +13,20 @@
 
 
 def relayout(stacked):
-    moved = lax.all_to_all(
-        lax.all_to_all(stacked, "tp", split_axis=1, concat_axis=2, tiled=True),
-        "fs",
-        split_axis=2,
-        concat_axis=1,
-        tiled=True,
+    moved = jnp.concatenate(
+        lax.all_to_all(
+            jnp.stack(
+                jnp.split(
+                    lax.all_to_all(stacked, "tp", split_axis=1, concat_axis=2, tiled=True),
+                    lax.axis_size("fs"),
+                    axis=2,
+                )
+            ),
+            "fs",
+            0,
+            0,
+        ),
+        axis=1,
     )
     whole = lax.all_gather(moved, ("gr", "tp"), axis=1, tiled=True)
     matrices = stacked.shape[0]

time: 615 us -> 561 us (0.912); the launches traced: 608 us -> 560 us
  local copies, waits for them, and re-layouts: 128 us -> 70.8 us
  blocking collectives: 138 us -> 147 us
    unnamed x16 -> x28, local copies, waits for them, and re-layouts: 55.2 us -> 30.2 us
    all_to_all x2 -> x0, local copies, waits for them, and re-layouts: 18.8 us -> none  [relayout(): lax.all_to_all(lax.all_to_all(stacked, 'tp', split_axis=1, concat_axis=2,...]
    all_to_all x4, local copies, waits for them, and re-layouts: 32.4 us -> 15.5 us  [relayout(): lax.all_to_all(stacked, 'tp', split_axis=1, concat_axis=2, tiled=True)]
    all_to_all x2, blocking collectives: 126 us -> 135 us  [relayout(): lax.all_to_all(jnp.stack(jnp.split(lax.all_to_all(stacked, 'tp', split_ax...]
  transfers between devices with their start and end apart: 6 -> 6, of which waited for: 5 -> 5; matrix products, arithmetic and copies ran while one was open for 16% -> 11% of each run, Pallas kernels for 0% -> 0%
where the time goes in v1:
time: 561 us; the launch traced here: 560 us
  waiting for transfers between devices  278 us (50%)
  blocking collectives  147 us (26%)
  local copies, waits for them, and re-layouts  70.8 us (13%)
  matrix products  37.2 us (7%)
  between operations  14.3 us (3%)
  other arithmetic  11.8 us (2%)
    all_to_all x2, blocking collectives, relayout(): lax.all_to_all(jnp.stack(jnp.split(lax.all_to_all(stacked, 'tp', split_ax...  135 us
    all_gather x2, waiting for transfers between devices, relayout(): whole = lax.all_gather(moved, ('gr', 'tp'), axis=1, tiled=True)  121 us
    all_gather x2, waiting for transfers between devices, half_step(): tokens_in = lax.all_gather(normed, 'fs', axis=0, tiled=True)  108 us
    reduce_scatter x2, waiting for transfers between devices, half_step(): lax.psum_scatter((lax.dot_general(hidden, down_weight, (((1,), (1,)), (()...  49.3 us
    unnamed x28, local copies, waits for them, and re-layouts  30.2 us
    dot_general x2, matrix products, half_step(): lax.dot_general(hidden, down_weight, (((1,), (1,)), ((), ())), preferred_...  24.9 us
    all_to_all x4, local copies, waits for them, and re-layouts, relayout(): lax.all_to_all(stacked, 'tp', split_axis=1, concat_axis=2, tiled=True)  15.5 us
    dot_general x2, matrix products, half_step(): jnp.dot(tokens_in, gate_weight, preferred_element_type=jnp.float32)  12.3 us
  transfers between devices with their start and end apart: 6, of which 5 were waited for; matrix products, arithmetic and copies ran while one was open for 11% of the time, Pallas kernels for 0%

profile of v1, /device:TPU:0, one launch (start us, length us, event | category | flops | bytes accessed | tf_op | source)
XLA Modules:
  0.0 559.7 jit_solution(983472712786277361)
XLA Ops:
  7.2 0.0 all-gather.5.cloned.1.call-start
  7.2 2.5 fusion.6
  9.7 0.2 pad_maximum_fusion
  10.0 1.9 copy.50
  11.8 6.0 %all_to_all.46 = bf16[3,128,2816]{2,0,1:T(4,128)(2,1)S(1)} all-to-all(bf16[3,128,2816]{2,0,1:T(4,128)(2,1)S(1)} %copy.50), channel_id=1, replica_groups=mesh['gr'=2,'fs'=8,'tp'=2] {'tp'}, dimensions={1} | all-to-all | bytes 4325376 | tf_op jit(solution)/shard_map/all_to_all | solution.py:20
  17.9 3.9 copy.71
  21.8 3.2 all_to_all.35
  25.1 0.1 fusion.24
  25.2 0.1 fusion.22
  25.4 0.1 fusion.20
  25.6 0.1 fusion.18
  25.8 61.2 %all_to_all.47 = bf16[8,3,64,704]{3,2,1,0:T(8,128)(2,1)S(1)} all-to-all(bf16[8,3,64,704]{3,2,1,0:T(8,128)(2,1)S(1)} %fusion.18), channel_id=1, replica_groups=mesh['gr'=2,'fs'=8,'tp'=2] {'fs'}, dimensions={0} | all-to-all | bytes 4325376 | tf_op jit(solution)/shard_map/all_to_all | solution.py:17
  87.0 1.6 copy.52
  88.6 0.0 all-gather.5.cloned.1.call-update
  88.6 0.0 all-gather.9.cloned.1.call-start
  88.7 0.9 copy-done.1
  89.6 0.2 fusion
  89.8 0.9 fusion.1
  90.7 0.2 reduce-scatter.3.cloned.1.call-start
  90.9 61.1 %all-gather.5.cloned.1.call-done = bf16[3,2048,704]{2,1,0:T(8,128)(2,1)} async-done(((bf16[3,512,704]{2,1,0:T(8,128)(2,1)}), bf16[3,2048,704]{2,1,0:T(8,128)(2,1)}) %all-gather.5.cloned.1.call-update) | async-done | bytes 8650768 | tf_op jit(solution)/shard_map/all_gather | solution.py:31
  152.1 4.1 fusion.31
  156.2 0.2 copy.53
  156.4 1.9 copy.54
  158.3 1.8 copy.55
  160.1 54.8 %all-gather.9.cloned.1.call-done = bf16[768,2048]{1,0:T(8,128)(2,1)} async-done(((bf16[96,2048]{1,0:T(8,128)(2,1)}), bf16[768,2048]{1,0:T(8,128)(2,1)}) %all-gather.9.cloned.1.call-update) | async-done | bytes 3145744 | tf_op jit(solution)/shard_map/all_gather | solution.py:54
  214.9 5.7 %fusion.32 = f32[768,704]{0,1:T(8,128)} fusion(bf16[768,2048]{1,0:T(8,128)(2,1)} %all-gather.9.cloned.1.call-done, bf16[2048,704]{1,0:T(8,128)(2,1)S(1)} %bitcast.110), kind=kOutput, calls=%fused_computation.70 | convolution fusion | flops 2214592512 | bytes 8192000 | tf_op jit(solution)/shard_map/dot_general | solution.py:55
  220.6 12.5 %multiply_convert_fusion.1 = bf16[768,2048]{1,0:T(8,128)(2,1)} fusion(bf16[2048,704]{1,0:T(8,128)(2,1)} %bitcast.114, f32[768,704]{0,1:T(8,128)} %fusion.32, bf16[768,2048]{1,0:T(8,128)(2,1)} %all-gather.9.cloned.1.call-done, bf16[2048,704]{1,0:T(8,128)(2,1)} %bitcast.112), kind=kOutput, calls=%fused_computation.1 | convolution fusion | flops 4436656128 | bytes 14221312 | tf_op jit(solution)/shard_map/dot_general | solution.py:60
  233.1 0.3 all-gather.7.cloned.1.call-start
  233.3 0.4 copy-done.3
  233.7 2.5 fusion.8
  236.2 0.2 pad_maximum_fusion.1
  236.4 1.9 copy.56
  238.3 6.0 %all_to_all.48 = bf16[3,128,2816]{2,0,1:T(4,128)(2,1)S(1)} all-to-all(bf16[3,128,2816]{2,0,1:T(4,128)(2,1)S(1)} %copy.56), channel_id=1, replica_groups=mesh['gr'=2,'fs'=8,'tp'=2] {'tp'}, dimensions={1} | all-to-all | bytes 4325376 | tf_op jit(solution)/shard_map/all_to_all | solution.py:20
  244.3 3.9 copy.70
  248.3 4.4 all_to_all.40
  252.7 1.1 fusion.17
  253.8 1.1 fusion.16
  255.0 1.0 fusion.15
  256.0 1.1 fusion.14
  257.2 0.1 fusion.12
  257.4 0.1 fusion.10
  257.5 73.3 %all_to_all.49 = bf16[8,3,64,704]{3,2,1,0:T(8,128)(2,1)S(1)} all-to-all(bf16[8,3,64,704]{3,2,1,0:T(8,128)(2,1)S(1)} %fusion.10), channel_id=1, replica_groups=mesh['gr'=2,'fs'=8,'tp'=2] {'fs'}, dimensions={0} | all-to-all | bytes 4325376 | tf_op jit(solution)/shard_map/all_to_all | solution.py:17
  330.8 1.6 copy.58
  332.5 0.0 all-gather.11.cloned.1.call-start
  332.5 0.0 reduce-scatter.3.cloned.1.call-done
  332.5 1.3 fusion.3
  333.8 1.9 fusion.4
  335.7 0.3 reduce-scatter.5.cloned.1.call-start
  336.0 60.0 %all-gather.7.cloned.1.call-done = bf16[3,2048,704]{2,1,0:T(8,128)(2,1)} async-done(((bf16[3,512,704]{2,1,0:T(8,128)(2,1)}), bf16[3,2048,704]{2,1,0:T(8,128)(2,1)}) %all-gather.7.cloned.1.call-update) | async-done | bytes 8650768 | tf_op jit(solution)/shard_map/all_gather | solution.py:31
  396.0 4.1 fusion.30
  400.1 1.9 copy.59
  402.0 1.9 copy.60
  403.9 1.9 copy.61
  405.8 52.8 %all-gather.11.cloned.1.call-done = bf16[768,2048]{1,0:T(8,128)(2,1)} async-done(((bf16[96,2048]{1,0:T(8,128)(2,1)}), bf16[768,2048]{1,0:T(8,128)(2,1)}) %all-gather.11.cloned.1.call-update) | async-done | bytes 3145744 | tf_op jit(solution)/shard_map/all_gather | solution.py:54
  458.7 6.6 %fusion.33 = f32[768,704]{0,1:T(8,128)} fusion(bf16[768,2048]{1,0:T(8,128)(2,1)} %all-gather.11.cloned.1.call-done, bf16[2048,704]{1,0:T(8,128)(2,1)} %bitcast.116), kind=kOutput, calls=%fused_computation.71 | convolution fusion | flops 2214592512 | bytes 8192000 | tf_op jit(solution)/shard_map/dot_general | solution.py:55
  465.3 12.4 %multiply_convert_fusion = bf16[768,2048]{1,0:T(8,128)(2,1)} fusion(bf16[2048,704]{1,0:T(8,128)(2,1)} %bitcast.120, f32[768,704]{0,1:T(8,128)} %fusion.33, bf16[768,2048]{1,0:T(8,128)(2,1)} %all-gather.11.cloned.1.call-done, bf16[2048,704]{1,0:T(8,128)(2,1)} %bitcast.118), kind=kOutput, calls=%fused_computation | convolution fusion | flops 4436656128 | bytes 14221312 | tf_op jit(solution)/shard_map/dot_general | solution.py:60
  477.7 4.6 copy.65
  482.3 4.6 copy.66
  486.9 4.6 copy.67
  491.4 2.7 copy.62
  494.1 4.7 copy.63
  498.9 2.7 copy.64
  501.5 49.3 %reduce-scatter.5.cloned.1.call-done = bf16[96,2048]{1,0:T(8,128)(2,1)} async-done(((bf16[768,2048]{1,0:T(8,128)(2,1)}), bf16[96,2048]{1,0:T(8,128)(2,1)}) %reduce-scatter.5.cloned.1.call-update) | async-done | bytes 393232 | tf_op jit(solution)/shard_map/reduce_scatter | solution.py:58
  550.8 2.1 fusion.5
  (19 shorter events, 0.2 us)
Async XLA Ops:
  7.2 144.9 %all-gather.5.cloned.1.call-start = ((), (), s32[]{:S(2)}) async-start(), calls=%async_computation.6 | async-start | bytes 11796480 | tf_op jit(solution)/shard_map/all_gather | solution.py:31
  88.6 1.0 copy-start.1
  88.6 126.2 %all-gather.9.cloned.1.call-start = ((), (), s32[]{:S(2)}) async-start(), calls=%async_computation.8 | async-start | bytes 3538944 | tf_op jit(solution)/shard_map/all_gather | solution.py:54
  90.7 241.8 %reduce-scatter.3.cloned.1.call-start = ((), (), s32[]{:S(2)}) async-start(), calls=%async_computation.9 | async-start | bytes 3538944 | tf_op jit(solution)/shard_map/reduce_scatter | solution.py:58
  233.0 0.7 copy-start.3
  233.1 162.9 %all-gather.7.cloned.1.call-start = ((), (), s32[]{:S(2)}) async-start(), calls=%async_computation.7 | async-start | bytes 11796480 | tf_op jit(solution)/shard_map/all_gather | solution.py:31
  252.7 4.4 copy-start.2
  332.5 126.2 %all-gather.11.cloned.1.call-start = ((), (), s32[]{:S(2)}) async-start(), calls=%async_computation.10 | async-start | bytes 3538944 | tf_op jit(solution)/shard_map/all_gather | solution.py:54
  335.7 215.1 %reduce-scatter.5.cloned.1.call-start = ((), (), s32[]{:S(2)}) async-start(), calls=%async_computation.11 | async-start | bytes 3538944 | tf_op jit(solution)/shard_map/reduce_scatter | solution.py:58
  494.1 4.7 copy-start
Sparse Core Ops, SparseCore 0:
  88.8 63.2 all-gather.4
  154.8 60.0 all-gather.8
  233.2 92.8 reduce-scatter.2
  332.6 63.3 all-gather.6
  398.6 60.0 all-gather.10
  477.9 72.9 reduce-scatter.4
